TPU v7x, 32 devices: a whole 2x2x4 slice. The times are simulated.
32 devices in a mesh: pp: 4 (over y, x), fs: 4 (over z), tp: 2 (over core).
Axes of the slice: x: 2, y: 2, z: 4, core: 2. Of those that a mesh axis runs over, the one named last changes fastest.
Arguments:
- micro_in: bfloat16 [2, 96, 1024], P(None, 'pp', ('tp', 'fs')), may hold values from -6 to 6
- norm_gain: float32 [4, 1024], P('pp'), may hold values from 0.5 to 1.5
- proj_gate: bfloat16 [4, 1024, 8, 4, 64], P('pp', None, 'tp', 'fs'), may hold values from -0.1875 to 0.1875
- proj_value: bfloat16 [4, 1024, 8, 4, 64], P('pp', None, 'tp', 'fs'), may hold values from -0.1875 to 0.1875
- proj_write: bfloat16 [4, 1024, 8, 128], P('pp', None, 'tp'), may hold values from -0.1875 to 0.1875
- proj_read: bfloat16 [4, 1024, 8, 128], P('pp', None, 'tp'), may hold values from -0.1875 to 0.1875
- proj_step: bfloat16 [4, 1024, 2, 8, 4], P('pp', None, None, 'tp', 'fs'), may hold values from -0.1875 to 0.1875
- step_bias: float32 [4, 2, 8, 4], P('pp', None, 'tp', 'fs'), may hold values from -4.6 to -2.3
- decay_log: float32 [4, 2, 8, 4], P('pp', None, 'tp', 'fs'), may hold values from 0 to 2.77
- skip_gain: float32 [4, 8, 4], P('pp', 'tp', 'fs'), may hold values from 0.5 to 1.5
- conv_value: float32 [4, 5, 8, 4, 64], P('pp', None, 'tp', 'fs'), may hold values from -2.5 to 2.5
- conv_write: float32 [4, 5, 8, 128], P('pp', None, 'tp'), may hold values from -2.5 to 2.5
- conv_read: float32 [4, 5, 8, 128], P('pp', None, 'tp'), may hold values from -2.5 to 2.5
- proj_out: bfloat16 [4, 8, 4, 64, 1024], P('pp', 'tp', 'fs'), may hold values from -0.125 to 0.125
Outputs:
- mixed_out: bfloat16 [2, 96, 1024], P(None, 'pp', ('tp', 'fs'))
All inputs are finite; a program needn't handle non-finite values.
Results may differ from a plain program's by a relative error of at most 0.025.
Values may be sent and summed in bfloat16 or wider, within the bound.
A program may use at most 64 MiB of HBM per device.

v0:
```python
import jax
import jax.numpy as jnp
from jax import lax
from jax.sharding import PartitionSpec as P

epsilon = 1e-06


def own_rows_2(portion, span, axis):
    count = span * lax.axis_size(axis)
    sent = portion(jnp.int32(0), count).astype(jnp.bfloat16)
    return lax.psum_scatter(sent, axis, scatter_dimension=0, tiled=True).astype(jnp.float32)


def from_behind(block, axis, distance):
    devices = range(lax.axis_size(axis))
    route = [(i - distance, i) for i in devices if i - distance in devices]
    return lax.ppermute(block, axis, route)


def spread(value, axis, source):
    kept = jnp.where(lax.axis_index(axis) == source, value, 0).astype(value.dtype)
    return lax.psum(kept, axis)


def centred_conv(signal, conv_taps):
    span_width = conv_taps.shape[0]
    half_width = span_width // 2
    length = signal.shape[0]
    padded = jnp.pad(signal, ((half_width, half_width), (0, 0)))
    running = jnp.zeros_like(signal)
    for offset in range(span_width):
        running = running + padded[offset : offset + length] * conv_taps[offset]
    return running


def duality_mix(
    gate_flat,
    value_flat,
    write_flat,
    read_flat,
    step_raw,
    step_bias,
    decay_log,
    skip_gain,
    conv_value,
    conv_write,
    conv_read,
):
    groups, per_group = skip_gain.shape
    length = gate_flat.shape[0]
    head_size = value_flat.shape[1] // (groups * per_group)
    state_size = write_flat.shape[1] // groups
    taps_count = conv_value.shape[0]
    value_act = jax.nn.silu(
        centred_conv(value_flat.astype(jnp.float32), conv_value.reshape(taps_count, -1))
    ).astype(jnp.bfloat16)
    write_act = jax.nn.silu(
        centred_conv(write_flat.astype(jnp.float32), conv_write.reshape(taps_count, -1))
    ).astype(jnp.bfloat16)
    read_act = jax.nn.silu(
        centred_conv(read_flat.astype(jnp.float32), conv_read.reshape(taps_count, -1))
    ).astype(jnp.bfloat16)
    step_size = jax.nn.softplus(step_raw.reshape(length, 2, groups, per_group) + step_bias[None])
    log_decay = step_size * (-jnp.exp(decay_log))[None]
    fwd_cum = jnp.cumsum(log_decay[:, 0], axis=0)
    bwd_cum = jnp.flip(jnp.cumsum(jnp.flip(log_decay[:, 1], 0), axis=0), 0)
    positions = jnp.arange(length)
    lower_mask = (positions[:, None] >= positions[None, :])[:, :, None, None]
    upper_mask = (positions[:, None] <= positions[None, :])[:, :, None, None]
    fwd_weight = (
        jnp.exp(jnp.where(lower_mask, fwd_cum[:, None] - fwd_cum[None, :], -jnp.inf))
        * step_size[None, :, 0]
    )
    bwd_weight = (
        jnp.exp(jnp.where(upper_mask, bwd_cum[:, None] - bwd_cum[None, :], -jnp.inf))
        * step_size[None, :, 1]
    )
    scores = jnp.einsum(
        "tgn,sgn->tsg",
        read_act.reshape(length, groups, state_size),
        write_act.reshape(length, groups, state_size),
        preferred_element_type=jnp.float32,
    )
    combined = scores[:, :, :, None] * (fwd_weight + bwd_weight)
    value_heads = value_act.reshape(length, groups, per_group, head_size).astype(jnp.float32)
    mixed_heads = jnp.einsum(
        "tsgh,sghp->tghp", combined, value_heads, precision=lax.Precision.HIGHEST
    )
    mixed_heads = mixed_heads + skip_gain[None, :, :, None] * value_heads
    return (mixed_heads.reshape(length, -1) * jax.nn.silu(gate_flat.astype(jnp.float32))).astype(
        jnp.bfloat16
    )


def body(
    micro_in,
    norm_gain,
    proj_gate,
    proj_value,
    proj_write,
    proj_read,
    proj_step,
    step_bias,
    decay_log,
    skip_gain,
    conv_value,
    conv_write,
    conv_read,
    proj_out,
):
    section_count = lax.axis_size("pp")
    section_idx = lax.axis_index("pp")
    width_model = norm_gain.shape[1]
    fed_blocks = lax.all_gather(micro_in, "pp", axis=1, tiled=True)
    micro_count = fed_blocks.shape[0]
    length = fed_blocks.shape[1]
    fed_columns = jnp.swapaxes(fed_blocks, 1, 2)
    gain_vec = norm_gain[0].astype(jnp.float32)
    cut_gate = proj_gate.shape[2] * proj_gate.shape[3] * proj_gate.shape[4]
    cut_write = proj_write.shape[2] * proj_write.shape[3]
    weight_all = jnp.concatenate(
        [
            proj_gate[0].reshape(width_model, -1),
            proj_value[0].reshape(width_model, -1),
            proj_write[0].reshape(width_model, -1),
            proj_read[0].reshape(width_model, -1),
            proj_step[0].reshape(width_model, -1),
        ],
        axis=1,
    )
    out_weights = proj_out[0].reshape(-1, width_model)
    own_rows = width_model // lax.axis_size(("tp", "fs"))

    def project(column_block):
        gathered = lax.all_gather(column_block, ("tp", "fs"), axis=0, tiled=True)
        as_float = gathered.astype(jnp.float32)
        scale_rms = lax.rsqrt(jnp.mean(as_float * as_float, axis=0) + epsilon)
        normed = (as_float * scale_rms[None, :] * gain_vec[:, None]).astype(jnp.bfloat16)
        return lax.dot_general(
            normed, weight_all, (((0,), (0,)), ((), ())), preferred_element_type=jnp.float32
        )

    def term_maker(token_rows):

        def term_rows(offset, span_count):
            weight_cols = lax.dynamic_slice_in_dim(out_weights, offset, span_count, 1)
            return lax.dot_general(
                weight_cols,
                token_rows,
                (((0,), (1,)), ((), ())),
                preferred_element_type=jnp.float32,
            )

        return term_rows

    def mix_block(column_block):
        projected = project(column_block)
        gate_flat = projected[:, :cut_gate].astype(jnp.bfloat16)
        value_flat = projected[:, cut_gate : 2 * cut_gate].astype(jnp.bfloat16)
        write_flat = projected[:, 2 * cut_gate : 2 * cut_gate + cut_write].astype(jnp.bfloat16)
        read_flat = projected[:, 2 * cut_gate + cut_write : 2 * cut_gate + 2 * cut_write].astype(
            jnp.bfloat16
        )
        step_raw = projected[:, 2 * cut_gate + 2 * cut_write :]
        gated_out = duality_mix(
            gate_flat,
            value_flat,
            write_flat,
            read_flat,
            step_raw,
            step_bias[0],
            decay_log[0],
            skip_gain[0],
            conv_value[0],
            conv_write[0],
            conv_read[0],
        )
        summed = own_rows_2(term_maker(gated_out), own_rows, ("tp", "fs"))
        branch = lax.optimization_barrier(summed.astype(jnp.bfloat16))
        return (column_block.astype(jnp.float32) + 0.5 * branch.astype(jnp.float32)).astype(
            jnp.bfloat16
        )

    total_steps = micro_count + section_count - 1

    def advance(moment, loop_state):
        arriving, collected = loop_state
        pick_index = jnp.clip(moment, 0, micro_count - 1)
        fresh_block = lax.dynamic_index_in_dim(fed_columns, pick_index, 0, keepdims=False)
        current = jnp.where(section_idx == 0, fresh_block, arriving)
        produced = mix_block(current)
        slot_index = moment - section_idx
        keep_flag = (
            (section_idx == section_count - 1) & (slot_index >= 0) & (slot_index < micro_count)
        )
        slot_safe = jnp.clip(slot_index, 0, micro_count - 1)
        previous = lax.dynamic_index_in_dim(collected, slot_safe, 0, keepdims=False)
        collected = lax.dynamic_update_index_in_dim(
            collected, jnp.where(keep_flag, produced, previous), slot_safe, 0
        )
        arriving = from_behind(produced, "pp", 1)
        return (arriving, collected)

    start_loop = (jnp.zeros_like(fed_columns[0]), jnp.zeros_like(fed_columns))
    arriving, collected = lax.fori_loop(0, total_steps, advance, start_loop)
    shared = spread(collected, "pp", section_count - 1)
    token_share = length // section_count
    own_block = lax.dynamic_slice_in_dim(shared, section_idx * token_share, token_share, 2)
    as_float = own_block.astype(jnp.float32)
    partial_squares = jnp.sum(as_float * as_float, axis=1)
    total_squares = lax.psum(partial_squares, ("tp", "fs"))
    scale_rms = lax.rsqrt(total_squares / width_model + epsilon)
    result = (as_float * scale_rms[:, None, :]).astype(jnp.bfloat16)
    return jnp.swapaxes(result, 1, 2)


def solution(mesh):
    return jax.shard_map(
        body,
        mesh=mesh,
        in_specs=(
            P(None, "pp", ("tp", "fs")),
            P("pp", None),
            P("pp", None, "tp", "fs", None),
            P("pp", None, "tp", "fs", None),
            P("pp", None, "tp", None),
            P("pp", None, "tp", None),
            P("pp", None, None, "tp", "fs"),
            P("pp", None, "tp", "fs"),
            P("pp", None, "tp", "fs"),
            P("pp", "tp", "fs"),
            P("pp", None, "tp", "fs", None),
            P("pp", None, "tp", None),
            P("pp", None, "tp", None),
            P("pp", "tp", "fs", None, None),
        ),
        out_specs=P(None, "pp", ("tp", "fs")),
        check_vma=False,
    )
```

profile of v0, /device:TPU:1, one launch (start us, length us, event | category | flops | bytes accessed | tf_op | source)
XLA Modules:
  0.0 505.2 jit_solution(10900077778748892538)
XLA Ops:
  16.3 8.0 %all_gather.13 = bf16[2,96,128]{2,1,0:T(8,128)(2,1)} all-gather(bf16[2,24,128]{2,1,0:T(8,128)(2,1)S(1)} %copy-done.6), channel_id=1, replica_groups=mesh['pp'=4,'fs'=4,'tp'=2] {'pp'}, dimensions={1}, use_global_device_ids=true | all-gather | bytes 61440 | tf_op jit(solution)/shard_map/all_gather | solution.py:115
  25.6 438.8 %while.17 = (s32[]{:T(128)}, bf16[128,96]{0,1:T(8,128)(2,1)S(1)}, bf16[2,128,96]{1,2,0:T(8,128)(2,1)}, pred[]{:T(512)}, bf16[2,128,96]{1,2,0:T(8,128)(2,1)}, /*i...) while((s32[]{:T(128)}, bf16[128,96]{0,1:T(8,128)(2,1)S(1)}, ...), condition=%wide.region_5.6_spmd, body=%wide.region_0.5_spmd.sunk | while | flops 395120736 | bytes 11393579 | solution.py:206
  27.0 24.4 %all_gather.15 = bf16[1024,96]{0,1:T(8,128)(2,1)S(1)} all-gather(bf16[128,96]{0,1:T(8,128)(2,1)S(1)} %bitcast_select_fusion.3), channel_id=1, replica_groups=mesh['pp'=4,'fs'=4,'tp'=2] {'tp','fs'}, dimensions={0}, use_global_device_ids=true | all-gather | bytes 221184 | tf_op jit(solution)/shard_map/while/body/eval_jaxpr/all_gather | solution.py:136
  51.5 2.3 fusion.90
  77.5 29.5 %reduce-scatter.6.cloned.1.call-done = bf16[128,96]{1,0:T(8,128)(2,1)} async-done(((bf16[1024,96]{1,0:T(8,128)(2,1)}), bf16[128,96]{1,0:T(8,128)(2,1)}) %reduce-scatter.6.cloned.1.call-update) | async-done | bytes 24592 | tf_op jit(solution)/shard_map/while
  109.2 3.1 collective-permute-start
  114.6 22.9 %all_gather.15 = bf16[1024,96]{0,1:T(8,128)(2,1)S(1)} all-gather(bf16[128,96]{0,1:T(8,128)(2,1)S(1)} %bitcast_select_fusion.3), channel_id=1, replica_groups=mesh['pp'=4,'fs'=4,'tp'=2] {'tp','fs'}, dimensions={0}, use_global_device_ids=true | all-gather | bytes 221184 | tf_op jit(solution)/shard_map/while/body/eval_jaxpr/all_gather | solution.py:136
  137.6 2.3 fusion.90
  163.7 31.1 %reduce-scatter.6.cloned.1.call-done = bf16[128,96]{1,0:T(8,128)(2,1)} async-done(((bf16[1024,96]{1,0:T(8,128)(2,1)}), bf16[128,96]{1,0:T(8,128)(2,1)}) %reduce-scatter.6.cloned.1.call-update) | async-done | bytes 24592 | tf_op jit(solution)/shard_map/while
  197.0 3.1 collective-permute-start
  202.4 22.6 %all_gather.15 = bf16[1024,96]{0,1:T(8,128)(2,1)S(1)} all-gather(bf16[128,96]{0,1:T(8,128)(2,1)S(1)} %bitcast_select_fusion.3), channel_id=1, replica_groups=mesh['pp'=4,'fs'=4,'tp'=2] {'tp','fs'}, dimensions={0}, use_global_device_ids=true | all-gather | bytes 221184 | tf_op jit(solution)/shard_map/while/body/eval_jaxpr/all_gather | solution.py:136
  225.2 2.3 fusion.90
  251.3 31.2 %reduce-scatter.6.cloned.1.call-done = bf16[128,96]{1,0:T(8,128)(2,1)} async-done(((bf16[1024,96]{1,0:T(8,128)(2,1)}), bf16[128,96]{1,0:T(8,128)(2,1)}) %reduce-scatter.6.cloned.1.call-update) | async-done | bytes 24592 | tf_op jit(solution)/shard_map/while
  284.7 3.1 collective-permute-start
  290.1 22.8 %all_gather.15 = bf16[1024,96]{0,1:T(8,128)(2,1)S(1)} all-gather(bf16[128,96]{0,1:T(8,128)(2,1)S(1)} %bitcast_select_fusion.3), channel_id=1, replica_groups=mesh['pp'=4,'fs'=4,'tp'=2] {'tp','fs'}, dimensions={0}, use_global_device_ids=true | all-gather | bytes 221184 | tf_op jit(solution)/shard_map/while/body/eval_jaxpr/all_gather | solution.py:136
  313.0 2.3 fusion.90
  339.1 31.2 %reduce-scatter.6.cloned.1.call-done = bf16[128,96]{1,0:T(8,128)(2,1)} async-done(((bf16[1024,96]{1,0:T(8,128)(2,1)}), bf16[128,96]{1,0:T(8,128)(2,1)}) %reduce-scatter.6.cloned.1.call-update) | async-done | bytes 24592 | tf_op jit(solution)/shard_map/while
  372.5 3.1 collective-permute-start
  377.9 22.8 %all_gather.15 = bf16[1024,96]{0,1:T(8,128)(2,1)S(1)} all-gather(bf16[128,96]{0,1:T(8,128)(2,1)S(1)} %bitcast_select_fusion.3), channel_id=1, replica_groups=mesh['pp'=4,'fs'=4,'tp'=2] {'tp','fs'}, dimensions={0}, use_global_device_ids=true | all-gather | bytes 221184 | tf_op jit(solution)/shard_map/while/body/eval_jaxpr/all_gather | solution.py:136
  400.8 2.3 fusion.90
  426.9 31.3 %reduce-scatter.6.cloned.1.call-done = bf16[128,96]{1,0:T(8,128)(2,1)} async-done(((bf16[1024,96]{1,0:T(8,128)(2,1)}), bf16[128,96]{1,0:T(8,128)(2,1)}) %reduce-scatter.6.cloned.1.call-update) | async-done | bytes 24592 | tf_op jit(solution)/shard_map/while
  460.3 3.1 collective-permute-start
  464.3 14.2 %psum.14 = bf16[2,128,96]{1,2,0:T(8,128)(2,1)S(1)} all-reduce(bf16[2,128,96]{1,2,0:T(8,128)(2,1)S(1)} %broadcast_select_fusion), channel_id=1, replica_groups=mesh['pp'=4,'fs'=4,'tp'=2] {'pp'}, use_global_device_ids=true, to_apply=%region_6.7 | all-reduce | flops 24576 | bytes 98304 | tf_op jit(solution)/shard_map/psum | solution.py:23
  478.7 19.4 %psum.15 = f32[2,24]{1,0:T(2,128)S(1)} all-reduce(f32[2,24]{1,0:T(2,128)S(1)} %fusion.49), channel_id=1, replica_groups=mesh['pp'=4,'fs'=4,'tp'=2] {'tp','fs'}, use_global_device_ids=true, to_apply=%region_8.9 | all-reduce | flops 48 | bytes 384 | tf_op jit(solution)/shard_map/psum | solution.py:212
  (259 shorter events, 153.5 us)
Async XLA Ops:
  9.6 4.8 copy-start.5
  9.7 6.7 %copy-start.6 = (bf16[2,24,128]{2,1,0:T(8,128)(2,1)S(1)}, bf16[2,24,128]{2,1,0:T(8,128)(2,1)}, u32[]{:S(2)}) copy-start(bf16[2,24,128]{2,1,0:T(8,128)(2,1)} %param.16) | copy-start | bytes 36868
  9.7 14.7 %copy-start.7 = (f32[1,2,4,1]{2,3,1,0:T(1,128)S(1)}, f32[1,2,4,1]{2,3,1,0:T(1,128)}, u32[]{:S(2)}) copy-start(f32[1,2,4,1]{2,3,1,0:T(1,128)} %param.24) | copy-start | bytes 100
  25.6 81.4 %reduce-scatter.6.cloned.1.call-start = ((), (), s32[]{:S(2)}) async-start(), calls=%async_computation.1 | async-start | bytes 294912 | tf_op jit(solution)/shard_map/while
  27.0 24.5 %copy-start.3 = (bf16[128,96]{0,1:T(8,128)(2,1)}, bf16[128,96]{0,1:T(8,128)(2,1)S(1)}, u32[]{:S(2)}) copy-start(bf16[128,96]{0,1:T(8,128)(2,1)S(1)} %bitcast_select_fusion.3) | copy-start | bytes 73732 | tf_op jit(solution)/shard_map/while
  68.2 3.1 copy-start.1
  68.2 3.1 copy-start.2
  109.2 4.0 collective-permute-start
  113.2 81.6 %reduce-scatter.6.cloned.1.call-start = ((), (), s32[]{:S(2)}) async-start(), calls=%async_computation.1 | async-start | bytes 294912 | tf_op jit(solution)/shard_map/while
  114.6 23.0 %copy-start.3 = (bf16[128,96]{0,1:T(8,128)(2,1)}, bf16[128,96]{0,1:T(8,128)(2,1)S(1)}, u32[]{:S(2)}) copy-start(bf16[128,96]{0,1:T(8,128)(2,1)S(1)} %bitcast_select_fusion.3) | copy-start | bytes 73732 | tf_op jit(solution)/shard_map/while
  154.4 3.1 copy-start.2
  197.0 4.0 collective-permute-start
  201.0 81.4 %reduce-scatter.6.cloned.1.call-start = ((), (), s32[]{:S(2)}) async-start(), calls=%async_computation.1 | async-start | bytes 294912 | tf_op jit(solution)/shard_map/while
  202.4 22.8 %copy-start.3 = (bf16[128,96]{0,1:T(8,128)(2,1)}, bf16[128,96]{0,1:T(8,128)(2,1)S(1)}, u32[]{:S(2)}) copy-start(bf16[128,96]{0,1:T(8,128)(2,1)S(1)} %bitcast_select_fusion.3) | copy-start | bytes 73732 | tf_op jit(solution)/shard_map/while
  242.0 3.1 copy-start.2
  284.7 4.0 collective-permute-start
  288.7 81.6 %reduce-scatter.6.cloned.1.call-start = ((), (), s32[]{:S(2)}) async-start(), calls=%async_computation.1 | async-start | bytes 294912 | tf_op jit(solution)/shard_map/while
  290.1 22.9 %copy-start.3 = (bf16[128,96]{0,1:T(8,128)(2,1)}, bf16[128,96]{0,1:T(8,128)(2,1)S(1)}, u32[]{:S(2)}) copy-start(bf16[128,96]{0,1:T(8,128)(2,1)S(1)} %bitcast_select_fusion.3) | copy-start | bytes 73732 | tf_op jit(solution)/shard_map/while
  329.8 3.1 copy-start.2
  372.5 4.0 collective-permute-start
  376.5 81.6 %reduce-scatter.6.cloned.1.call-start = ((), (), s32[]{:S(2)}) async-start(), calls=%async_computation.1 | async-start | bytes 294912 | tf_op jit(solution)/shard_map/while
  377.9 22.9 %copy-start.3 = (bf16[128,96]{0,1:T(8,128)(2,1)}, bf16[128,96]{0,1:T(8,128)(2,1)S(1)}, u32[]{:S(2)}) copy-start(bf16[128,96]{0,1:T(8,128)(2,1)S(1)} %bitcast_select_fusion.3) | copy-start | bytes 73732 | tf_op jit(solution)/shard_map/while
  417.6 3.1 copy-start.2
  460.3 4.0 collective-permute-start
  (10 other events, 19.4 us)
Sparse Core Ops, SparseCore 0:
  76.9 30.0 reduce-scatter.5
  163.0 31.6 reduce-scatter.5
  250.6 31.7 reduce-scatter.5
  338.4 31.7 reduce-scatter.5
  426.2 31.8 reduce-scatter.5
where the time goes:
time: 509 us; the launch traced here: 505 us
  waiting for transfers between devices  159 us (31%)
  blocking collectives  157 us (31%)
  local copies, waits for them, and re-layouts  86.1 us (17%)
  other arithmetic  37.1 us (7%)
  matrix products  37 us (7%)
  starting transfers between devices  15.4 us (3%)
  between operations  13.2 us (3%)
    while x10, waiting for transfers between devices  154 us
    all_gather x5, blocking collectives, project(): gathered = lax.all_gather(column_block, ('tp', 'fs'), axis=0, tiled=True)  115 us
    mul x30, local copies, waits for them, and re-layouts, centred_conv(): running = running + padded[offset:offset + length] * conv_taps[offset]  20.8 us
    psum x1, blocking collectives, body(): total_squares = lax.psum(partial_squares, ('tp', 'fs'))  19.4 us
    rev x20, local copies, waits for them, and re-layouts, duality_mix(): bwd_cum = jnp.flip(jnp.cumsum(jnp.flip(log_decay[:, 1], 0), axis=0), 0)  17.8 us
    ppermute x5, starting transfers between devices, from_behind(): return lax.ppermute(block, axis, route)  15.4 us
    psum x1, blocking collectives, spread(): return lax.psum(kept, axis)  14.2 us
    while x50, local copies, waits for them, and re-layouts  13.1 us
  transfers between devices with their start and end apart: 10, of which 10 were waited for; matrix products, arithmetic and copies ran while one was open for 1% of the time, Pallas kernels for 0%

commit v1 on v0

--- a/solution.py
+++ b/solution.py
@@ -133,7 +133,8 @@
     own_rows = width_model // lax.axis_size(("tp", "fs"))
 
     def project(column_block):
-        gathered = lax.all_gather(column_block, ("tp", "fs"), axis=0, tiled=True)
+        outgoing = jnp.stack([column_block] * lax.axis_size(("tp", "fs")))
+        gathered = jnp.concatenate(lax.all_to_all(outgoing, ("tp", "fs"), 0, 0), axis=0)
         as_float = gathered.astype(jnp.float32)
         scale_rms = lax.rsqrt(jnp.mean(as_float * as_float, axis=0) + epsilon)
         normed = (as_float * scale_rms[None, :] * gain_vec[:, None]).astype(jnp.bfloat16)

time: 509 us -> 441 us (0.87)
  blocking collectives: 157 us -> 41.5 us
  starting transfers between devices: 15.4 us -> 42.2 us
  waiting for transfers between devices: 159 us -> 182 us
    all_gather x5 -> x0, blocking collectives: 115 us -> none  [project(): gathered = lax.all_gather(column_block, ('tp', 'fs'), axis=0, tiled=True)]
    all_to_all x0 -> x5, starting transfers between devices: none -> 26.8 us  [project(): lax.all_to_all(outgoing, ('tp', 'fs'), 0, 0)]
    all_to_all x0 -> x5, waiting for transfers between devices: none -> 25.6 us  [project(): lax.all_to_all(outgoing, ('tp', 'fs'), 0, 0)]
    mul x30, local copies, waits for them, and re-layouts: 20.8 us -> 9.02 us  [centred_conv(): running = running + padded[offset:offset + length] * conv_taps[offset]]
  transfers between devices with their start and end apart: 10 -> 15, of which waited for: 10 -> 15; matrix products, arithmetic and copies ran while one was open for 1% -> 4% of each run, Pallas kernels for 0% -> 0%
where the time goes in v1:
time: 441 us; the launch traced here: 437 us
  waiting for transfers between devices  182 us (41%)
  local copies, waits for them, and re-layouts  83.8 us (19%)
  starting transfers between devices  42.2 us (10%)
  blocking collectives  41.5 us (9%)
  matrix products  38.3 us (9%)
  other arithmetic  35.4 us (8%)
  between operations  13.2 us (3%)
    while x10, waiting for transfers between devices  152 us
    all_to_all x5, starting transfers between devices, project(): lax.all_to_all(outgoing, ('tp', 'fs'), 0, 0)  26.8 us
    all_to_all x5, waiting for transfers between devices, project(): lax.all_to_all(outgoing, ('tp', 'fs'), 0, 0)  25.6 us
    psum x1, blocking collectives, body(): total_squares = lax.psum(partial_squares, ('tp', 'fs'))  19.3 us
    rev x20, local copies, waits for them, and re-layouts, duality_mix(): bwd_cum = jnp.flip(jnp.cumsum(jnp.flip(log_decay[:, 1], 0), axis=0), 0)  17.8 us
    while x50, local copies, waits for them, and re-layouts  16.1 us
    ppermute x5, starting transfers between devices, from_behind(): return lax.ppermute(block, axis, route)  15.3 us
    psum x1, blocking collectives, spread(): return lax.psum(kept, axis)  14.2 us
  transfers between devices with their start and end apart: 15, of which 15 were waited for; matrix products, arithmetic and copies ran while one was open for 4% of the time, Pallas kernels for 0%

profile of v1, /device:TPU:1, one launch (start us, length us, event | category | flops | bytes accessed | tf_op | source)
XLA Modules:
  0.0 436.7 jit_solution(9364202150992036408)
XLA Ops:
  16.4 8.0 %all_gather.3 = bf16[2,96,128]{2,1,0:T(8,128)(2,1)} all-gather(bf16[2,24,128]{2,1,0:T(8,128)(2,1)S(1)} %copy-done.8), channel_id=1, replica_groups=mesh['pp'=4,'fs'=4,'tp'=2] {'pp'}, dimensions={1}, use_global_device_ids=true | all-gather | bytes 61440 | tf_op jit(solution)/shard_map/all_gather | solution.py:115
  25.6 370.2 %while.17 = (s32[]{:T(128)}, bf16[128,96]{0,1:T(8,128)(2,1)S(1)}, bf16[2,128,96]{1,2,0:T(8,128)(2,1)}, pred[]{:T(512)}, bf16[2,128,96]{1,2,0:T(8,128)(2,1)}, /*i...) while((s32[]{:T(128)}, bf16[128,96]{0,1:T(8,128)(2,1)S(1)}, ...), condition=%wide.region_5.6_spmd, body=%wide.region_0.5_spmd.sunk | while | flops 395120736 | bytes 11988555 | solution.py:207
  27.7 7.2 %all-to-all-start = ((bf16[8,128,96]{1,2,0:T(8,128)(2,1)}), bf16[8,128,96]{1,2,0:T(8,128)(2,1)}, u32[]{:S(2)}, u32[]{:S(2)}) async-start(bf16[8,128,96]{1,2,0:T(8,128)(2,1)} %stack.7), calls=%async_computation | async-start | bytes 393216 | tf_op jit(solution)/shard_map/while/body/eval_jaxpr/all_to_all | solution.py:137
  37.5 5.1 %all-to-all-done = bf16[8,128,96]{1,2,0:T(8,128)(2,1)} async-done(((bf16[8,128,96]{1,2,0:T(8,128)(2,1)}), bf16[8,128,96]{1,2,0:T(8,128)(2,1)}, u32[]{:S(2)}, u32[]{:S(2)}) %all-to-all-start) | async-done | bytes 196640 | tf_op jit(solution)/shard_map/while/body/eval_jaxpr/all_to_all | solution.py:137
  65.0 28.9 %reduce-scatter.6.cloned.1.call-done = bf16[128,96]{1,0:T(8,128)(2,1)} async-done(((bf16[1024,96]{1,0:T(8,128)(2,1)}), bf16[128,96]{1,0:T(8,128)(2,1)}) %reduce-scatter.6.cloned.1.call-update) | async-done | bytes 24592 | tf_op jit(solution)/shard_map/while
  96.2 3.1 collective-permute-start
  102.2 4.9 %all-to-all-start = ((bf16[8,128,96]{1,2,0:T(8,128)(2,1)}), bf16[8,128,96]{1,2,0:T(8,128)(2,1)}, u32[]{:S(2)}, u32[]{:S(2)}) async-start(bf16[8,128,96]{1,2,0:T(8,128)(2,1)} %stack.7), calls=%async_computation | async-start | bytes 393216 | tf_op jit(solution)/shard_map/while/body/eval_jaxpr/all_to_all | solution.py:137
  109.8 5.1 %all-to-all-done = bf16[8,128,96]{1,2,0:T(8,128)(2,1)} async-done(((bf16[8,128,96]{1,2,0:T(8,128)(2,1)}), bf16[8,128,96]{1,2,0:T(8,128)(2,1)}, u32[]{:S(2)}, u32[]{:S(2)}) %all-to-all-start) | async-done | bytes 196640 | tf_op jit(solution)/shard_map/while/body/eval_jaxpr/all_to_all | solution.py:137
  137.3 30.6 %reduce-scatter.6.cloned.1.call-done = bf16[128,96]{1,0:T(8,128)(2,1)} async-done(((bf16[1024,96]{1,0:T(8,128)(2,1)}), bf16[128,96]{1,0:T(8,128)(2,1)}) %reduce-scatter.6.cloned.1.call-update) | async-done | bytes 24592 | tf_op jit(solution)/shard_map/while
  170.1 3.1 collective-permute-start
  176.1 4.9 %all-to-all-start = ((bf16[8,128,96]{1,2,0:T(8,128)(2,1)}), bf16[8,128,96]{1,2,0:T(8,128)(2,1)}, u32[]{:S(2)}, u32[]{:S(2)}) async-start(bf16[8,128,96]{1,2,0:T(8,128)(2,1)} %stack.7), calls=%async_computation | async-start | bytes 393216 | tf_op jit(solution)/shard_map/while/body/eval_jaxpr/all_to_all | solution.py:137
  183.6 5.1 %all-to-all-done = bf16[8,128,96]{1,2,0:T(8,128)(2,1)} async-done(((bf16[8,128,96]{1,2,0:T(8,128)(2,1)}), bf16[8,128,96]{1,2,0:T(8,128)(2,1)}, u32[]{:S(2)}, u32[]{:S(2)}) %all-to-all-start) | async-done | bytes 196640 | tf_op jit(solution)/shard_map/while/body/eval_jaxpr/all_to_all | solution.py:137
  211.1 30.6 %reduce-scatter.6.cloned.1.call-done = bf16[128,96]{1,0:T(8,128)(2,1)} async-done(((bf16[1024,96]{1,0:T(8,128)(2,1)}), bf16[128,96]{1,0:T(8,128)(2,1)}) %reduce-scatter.6.cloned.1.call-update) | async-done | bytes 24592 | tf_op jit(solution)/shard_map/while
  244.0 3.1 collective-permute-start
  250.0 4.9 %all-to-all-start = ((bf16[8,128,96]{1,2,0:T(8,128)(2,1)}), bf16[8,128,96]{1,2,0:T(8,128)(2,1)}, u32[]{:S(2)}, u32[]{:S(2)}) async-start(bf16[8,128,96]{1,2,0:T(8,128)(2,1)} %stack.7), calls=%async_computation | async-start | bytes 393216 | tf_op jit(solution)/shard_map/while/body/eval_jaxpr/all_to_all | solution.py:137
  257.6 5.1 %all-to-all-done = bf16[8,128,96]{1,2,0:T(8,128)(2,1)} async-done(((bf16[8,128,96]{1,2,0:T(8,128)(2,1)}), bf16[8,128,96]{1,2,0:T(8,128)(2,1)}, u32[]{:S(2)}, u32[]{:S(2)}) %all-to-all-start) | async-done | bytes 196640 | tf_op jit(solution)/shard_map/while/body/eval_jaxpr/all_to_all | solution.py:137
  285.1 30.6 %reduce-scatter.6.cloned.1.call-done = bf16[128,96]{1,0:T(8,128)(2,1)} async-done(((bf16[1024,96]{1,0:T(8,128)(2,1)}), bf16[128,96]{1,0:T(8,128)(2,1)}) %reduce-scatter.6.cloned.1.call-update) | async-done | bytes 24592 | tf_op jit(solution)/shard_map/while
  317.9 3.1 collective-permute-start
  324.0 4.9 %all-to-all-start = ((bf16[8,128,96]{1,2,0:T(8,128)(2,1)}), bf16[8,128,96]{1,2,0:T(8,128)(2,1)}, u32[]{:S(2)}, u32[]{:S(2)}) async-start(bf16[8,128,96]{1,2,0:T(8,128)(2,1)} %stack.7), calls=%async_computation | async-start | bytes 393216 | tf_op jit(solution)/shard_map/while/body/eval_jaxpr/all_to_all | solution.py:137
  331.5 5.1 %all-to-all-done = bf16[8,128,96]{1,2,0:T(8,128)(2,1)} async-done(((bf16[8,128,96]{1,2,0:T(8,128)(2,1)}), bf16[8,128,96]{1,2,0:T(8,128)(2,1)}, u32[]{:S(2)}, u32[]{:S(2)}) %all-to-all-start) | async-done | bytes 196640 | tf_op jit(solution)/shard_map/while/body/eval_jaxpr/all_to_all | solution.py:137
  359.0 30.6 %reduce-scatter.6.cloned.1.call-done = bf16[128,96]{1,0:T(8,128)(2,1)} async-done(((bf16[1024,96]{1,0:T(8,128)(2,1)}), bf16[128,96]{1,0:T(8,128)(2,1)}) %reduce-scatter.6.cloned.1.call-update) | async-done | bytes 24592 | tf_op jit(solution)/shard_map/while
  391.8 3.1 collective-permute-start
  395.8 14.2 %psum.14 = bf16[2,128,96]{1,2,0:T(8,128)(2,1)S(1)} all-reduce(bf16[2,128,96]{1,2,0:T(8,128)(2,1)S(1)} %broadcast_select_fusion), channel_id=1, replica_groups=mesh['pp'=4,'fs'=4,'tp'=2] {'pp'}, use_global_device_ids=true, to_apply=%region_6.7 | all-reduce | flops 24576 | bytes 98304 | tf_op jit(solution)/shard_map/psum | solution.py:23
  410.2 19.3 %psum.15 = f32[2,24]{1,0:T(2,128)S(1)} all-reduce(f32[2,24]{1,0:T(2,128)S(1)} %fusion.49), channel_id=1, replica_groups=mesh['pp'=4,'fs'=4,'tp'=2] {'tp','fs'}, use_global_device_ids=true, to_apply=%region_8.9 | all-reduce | flops 48 | bytes 384 | tf_op jit(solution)/shard_map/psum | solution.py:213
  (273 shorter events, 162.1 us)
Async XLA Ops:
  9.6 4.8 %copy-start.7 = (bf16[1,1024,2,4,1]{1,3,4,2,0:T(4,128)(2,1)S(1)}, bf16[1,1024,2,4,1]{1,3,4,2,0:T(4,128)(2,1)}, u32[]{:S(2)}) copy-start(bf16[1,1024,2,4,1]{1,3,4,2,0:T(4,128)(2,1)} %param.22) | copy-start | bytes 49156
  9.7 6.7 %copy-start.8 = (bf16[2,24,128]{2,1,0:T(8,128)(2,1)S(1)}, bf16[2,24,128]{2,1,0:T(8,128)(2,1)}, u32[]{:S(2)}) copy-start(bf16[2,24,128]{2,1,0:T(8,128)(2,1)} %param.16) | copy-start | bytes 36868
  9.7 14.7 %copy-start.9 = (f32[1,2,4,1]{2,3,1,0:T(1,128)S(1)}, f32[1,2,4,1]{2,3,1,0:T(1,128)}, u32[]{:S(2)}) copy-start(f32[1,2,4,1]{2,3,1,0:T(1,128)} %param.24) | copy-start | bytes 100
  9.7 15.9 %copy-start.5 = (f32[1,5,4,128]{3,2,1,0:T(4,128)S(1)}, f32[1,5,4,128]{3,2,1,0:T(4,128)}, u32[]{:S(2)}) copy-start(f32[1,5,4,128]{3,2,1,0:T(4,128)} %param.27) | copy-start | bytes 30724
  9.7 15.9 %copy-start.6 = (f32[1,1024]{1,0:T(1,128)S(1)}, f32[1,1024]{1,0:T(1,128)}, u32[]{:S(2)}) copy-start(f32[1,1024]{1,0:T(1,128)} %param.17) | copy-start | bytes 12292
  11.8 2.6 copy-start.4
  27.7 15.0 %all-to-all-start = ((bf16[8,128,96]{1,2,0:T(8,128)(2,1)}), bf16[8,128,96]{1,2,0:T(8,128)(2,1)}, u32[]{:S(2)}, u32[]{:S(2)}) async-start(bf16[8,128,96]{1,2,0:T(8,128)(2,1)} %stack.7), calls=%async_computation | async-start | bytes 393216 | tf_op jit(solution)/shard_map/while/body/eval_jaxpr/all_to_all | solution.py:137
  34.9 59.0 %reduce-scatter.6.cloned.1.call-start = ((), (), s32[]{:S(2)}) async-start(), calls=%async_computation.2 | async-start | bytes 294912 | tf_op jit(solution)/shard_map/while
  56.6 2.3 copy-start.2
  96.2 4.0 collective-permute-start
  102.2 12.6 %all-to-all-start = ((bf16[8,128,96]{1,2,0:T(8,128)(2,1)}), bf16[8,128,96]{1,2,0:T(8,128)(2,1)}, u32[]{:S(2)}, u32[]{:S(2)}) async-start(bf16[8,128,96]{1,2,0:T(8,128)(2,1)} %stack.7), calls=%async_computation | async-start | bytes 393216 | tf_op jit(solution)/shard_map/while/body/eval_jaxpr/all_to_all | solution.py:137
  107.1 60.7 %reduce-scatter.6.cloned.1.call-start = ((), (), s32[]{:S(2)}) async-start(), calls=%async_computation.2 | async-start | bytes 294912 | tf_op jit(solution)/shard_map/while
  128.8 2.3 copy-start.2
  170.1 4.0 collective-permute-start
  176.1 12.6 %all-to-all-start = ((bf16[8,128,96]{1,2,0:T(8,128)(2,1)}), bf16[8,128,96]{1,2,0:T(8,128)(2,1)}, u32[]{:S(2)}, u32[]{:S(2)}) async-start(bf16[8,128,96]{1,2,0:T(8,128)(2,1)} %stack.7), calls=%async_computation | async-start | bytes 393216 | tf_op jit(solution)/shard_map/while/body/eval_jaxpr/all_to_all | solution.py:137
  181.0 60.8 %reduce-scatter.6.cloned.1.call-start = ((), (), s32[]{:S(2)}) async-start(), calls=%async_computation.2 | async-start | bytes 294912 | tf_op jit(solution)/shard_map/while
  202.7 2.3 copy-start.2
  244.0 4.0 collective-permute-start
  250.0 12.6 %all-to-all-start = ((bf16[8,128,96]{1,2,0:T(8,128)(2,1)}), bf16[8,128,96]{1,2,0:T(8,128)(2,1)}, u32[]{:S(2)}, u32[]{:S(2)}) async-start(bf16[8,128,96]{1,2,0:T(8,128)(2,1)} %stack.7), calls=%async_computation | async-start | bytes 393216 | tf_op jit(solution)/shard_map/while/body/eval_jaxpr/all_to_all | solution.py:137
  254.9 60.8 %reduce-scatter.6.cloned.1.call-start = ((), (), s32[]{:S(2)}) async-start(), calls=%async_computation.2 | async-start | bytes 294912 | tf_op jit(solution)/shard_map/while
  317.9 4.0 collective-permute-start
  324.0 12.6 %all-to-all-start = ((bf16[8,128,96]{1,2,0:T(8,128)(2,1)}), bf16[8,128,96]{1,2,0:T(8,128)(2,1)}, u32[]{:S(2)}, u32[]{:S(2)}) async-start(bf16[8,128,96]{1,2,0:T(8,128)(2,1)} %stack.7), calls=%async_computation | async-start | bytes 393216 | tf_op jit(solution)/shard_map/while/body/eval_jaxpr/all_to_all | solution.py:137
  328.9 60.8 %reduce-scatter.6.cloned.1.call-start = ((), (), s32[]{:S(2)}) async-start(), calls=%async_computation.2 | async-start | bytes 294912 | tf_op jit(solution)/shard_map/while
  391.8 4.0 collective-permute-start
  (17 other events, 23.4 us)
Sparse Core Ops, SparseCore 0:
  64.4 29.5 reduce-scatter.5
  136.6 31.1 reduce-scatter.5
  210.5 31.2 reduce-scatter.5
  284.4 31.2 reduce-scatter.5
  358.3 31.2 reduce-scatter.5
